TPU v7x, 32 devices: a whole 2x2x4 slice. The times are simulated.
32 devices in a mesh: ep: 8 (over z, x), tp: 4 (over y, core).
Axes of the slice: x: 2, y: 2, z: 4, core: 2. Of those that a mesh axis runs over, the one named last changes fastest.
Arguments:
- query_rows: bfloat16 [3072, 4096], P('ep', 'tp'), may hold values from -6 to 6
- key_rows: bfloat16 [3072, 2048], P('ep', 'tp'), may hold values from -6 to 6
- value_rows: bfloat16 [3072, 2048], P('ep', 'tp'), may hold values from -6 to 6
- query_gain: float32 [128], replicated, may hold values from 0.4 to 5
- key_gain: float32 [128], replicated, may hold values from 0.4 to 5
- w_out: bfloat16 [4096, 2048], P('tp'), may hold values from -0.09375 to 0.09375
- mixer_gain: float32 [2048], replicated, may hold values from 0.1 to 1.9
- expert_input: bfloat16 [1536, 2048], P('ep'), may hold values from -6 to 6
- expert_ids: int32 [1536, 2], P('ep'), may hold values from 0 to 7, as said below
- expert_weights: float32 [1536, 2], P('ep'), may hold values from 0.1 to 1
- input_gain: float32 [2048], replicated, may hold values from 0.1 to 1.9
- w_gate: bfloat16 [8, 2048, 4096], P('ep', None, 'tp'), may hold values from -0.125 to 0.125
- w_up: bfloat16 [8, 2048, 4096], P('ep', None, 'tp'), may hold values from -0.125 to 0.125
- w_down: bfloat16 [8, 4096, 2048], P('ep', 'tp'), may hold values from -2 to 2
- out_gain: float32 [2048], P('tp'), may hold values from 0.1 to 1.9
Outputs:
- mixer_result: bfloat16 [3072, 2048], P(('ep', 'tp'))
- moe_result: bfloat16 [1536, 2048], P('ep', 'tp')
Inputs may be any that keep to these rules, and one draw needn't show every extreme that they name: `expert_ids`: the two experts of a row differ and lie in one group of 2 consecutive experts. Among the rows of one index of ep (aligned blocks of 192 rows) no expert is named by more than 72 rows, and in every block some expert is named by exactly 72 rows.
All inputs are finite; a program needn't handle non-finite values.
Results may differ from a plain program's by a relative error of at most 0.02.
The roundings to bfloat16 on the way count: a program that leaves them out, or rounds other values in their place, can miss the bound.
Values may be sent and summed in bfloat16 or wider, within the bound.
A program may use at most 64 MiB of HBM per device.

v0:
```python
import jax
import jax.numpy as jnp
from jax import lax
from jax.sharding import PartitionSpec as P

D = 2048
GRID = 64
GROUPS = 4


EPS = 1e-06
THETA = 10000.0


def turn_half(half_part, position):
    half_width = half_part.shape[-1]
    frequency = THETA ** (-jnp.arange(0, half_width, 2, dtype=jnp.float32) / half_width)
    angles = position[:, None, None] * frequency[None, None, :]
    cosine = jnp.cos(angles)
    sine_part = jnp.sin(angles)
    first_half = half_part[..., : half_width // 2]
    second = half_part[..., half_width // 2 :]
    return jnp.concatenate(
        [first_half * cosine - second * sine_part, second * cosine + first_half * sine_part],
        axis=-1,
    )


def norm_turn(raw_rows, gain_vec, row_offset):
    row_count = raw_rows.shape[0]
    head_dim = gain_vec.shape[0]
    head_count = raw_rows.shape[1] // head_dim
    by_head = raw_rows.astype(jnp.float32).reshape(row_count, head_count, head_dim)
    scaled = (
        by_head * lax.rsqrt(jnp.mean(by_head * by_head, axis=-1, keepdims=True) + EPS) * gain_vec
    )
    position = row_offset + jnp.arange(row_count, dtype=jnp.int32)
    grid_row = (position // GRID).astype(jnp.float32)
    grid_col = (position % GRID).astype(jnp.float32)
    half_dim = head_dim // 2
    turned = jnp.concatenate(
        [turn_half(scaled[..., :half_dim], grid_row), turn_half(scaled[..., half_dim:], grid_col)],
        axis=-1,
    )
    return turned.reshape(row_count, head_count * head_dim).astype(jnp.bfloat16)


def mixer_half(query_rows, key_rows, value_rows, query_gain, key_gain, w_out, mixer_gain):
    row_count = query_rows.shape[0]
    head_dim = query_gain.shape[0]
    row_offset = lax.axis_index("ep") * row_count
    query_turned = norm_turn(query_rows, query_gain, row_offset)
    key_turned = norm_turn(key_rows, key_gain, row_offset)
    local_kv = key_rows.shape[1] // head_dim
    group_size = query_rows.shape[1] // key_rows.shape[1]
    lane_count = group_size * row_count
    grouped = (
        query_turned.reshape(row_count, local_kv, group_size, head_dim)
        .transpose(1, 2, 0, 3)
        .reshape(local_kv, lane_count, head_dim)
    )
    scaling = head_dim ** (-0.5)

    def attend_block(carry, block_pair):
        running_max, running_sum, weighted = carry
        key_block, value_block = block_pair
        scores = (
            jnp.einsum("gqd,ngd->gqn", grouped, key_block, preferred_element_type=jnp.float32)
            * scaling
        )
        new_max = jnp.maximum(running_max, jnp.max(scores, axis=-1))
        exponent = jnp.exp(scores - new_max[..., None])
        factor = jnp.exp(running_max - new_max)
        running_sum = running_sum * factor + jnp.sum(exponent, axis=-1)
        weighted = weighted * factor[..., None] + jnp.einsum(
            "gqn,ngd->gqd",
            exponent.astype(jnp.bfloat16),
            value_block,
            preferred_element_type=jnp.float32,
        )
        return ((new_max, running_sum, weighted), None)

    initial = (
        jnp.full((local_kv, lane_count), -1e30, jnp.float32),
        jnp.zeros((local_kv, lane_count), jnp.float32),
        jnp.zeros((local_kv, lane_count, head_dim), jnp.float32),
    )
    carry = initial
    key_piece = lax.all_gather(key_turned, "ep", axis=0, tiled=True)
    value_piece = lax.all_gather(value_rows, "ep", axis=0, tiled=True)
    piece_rows = key_piece.shape[0]
    block_rows = 512
    block_count = piece_rows // block_rows
    key_split = key_piece.reshape(block_count, block_rows, local_kv, head_dim)
    value_split = value_piece.reshape(block_count, block_rows, local_kv, head_dim)
    carry, _ = lax.scan(attend_block, carry, (key_split, value_split))
    running_max, running_sum, weighted = carry
    attended = (weighted / running_sum[..., None]).astype(jnp.bfloat16)
    attended = (
        attended.reshape(local_kv, group_size, row_count, head_dim)
        .transpose(2, 0, 1, 3)
        .reshape(row_count, local_kv * group_size * head_dim)
    )
    mixed_sum = lax.psum_scatter(
        jnp.dot(attended, w_out, preferred_element_type=jnp.float32).astype(jnp.bfloat16),
        "tp",
        scatter_dimension=0,
        tiled=True,
    ).astype(jnp.float32)
    scaled = (
        mixed_sum
        * lax.rsqrt(jnp.mean(mixed_sum * mixed_sum, axis=1, keepdims=True) + EPS)
        * mixer_gain
    )
    return scaled.astype(jnp.bfloat16)


def expert_half(
    expert_input, expert_ids, expert_weights, input_gain, w_gate, w_up, w_down, out_gain
):
    row_count = expert_input.shape[0]
    top_count = expert_ids.shape[1]
    expert_total = w_gate.shape[0] * lax.axis_size("ep")
    inner_count = expert_total // GROUPS
    capacity = 3 * row_count // (4 * inner_count)
    inputs_f = expert_input.astype(jnp.float32)
    normed = (
        inputs_f
        * lax.rsqrt(jnp.mean(inputs_f * inputs_f, axis=1, keepdims=True) + EPS)
        * input_gain
    ).astype(jnp.bfloat16)
    flat_ids = expert_ids.reshape(-1)
    one_hot = (flat_ids[:, None] == jnp.arange(expert_total, dtype=jnp.int32)[None, :]).astype(
        jnp.int32
    )
    earlier = jnp.cumsum(one_hot, axis=0) - one_hot
    rank_in = jnp.sum(earlier * one_hot, axis=1)
    slot_of = flat_ids * capacity + rank_in
    pick_rows = jnp.arange(flat_ids.shape[0], dtype=jnp.int32) // top_count
    source_row = (
        jnp.full((expert_total * capacity,), row_count, jnp.int32).at[slot_of].set(pick_rows)
    )
    padded = jnp.concatenate([normed, jnp.zeros((1, normed.shape[1]), jnp.bfloat16)], axis=0)
    gate_local = w_gate[0]
    up_local = w_up[0]
    down_local = w_down[0]
    outgoing = jnp.take(padded, source_row, axis=0)
    arrived = lax.all_to_all(outgoing, "ep", split_axis=0, concat_axis=0, tiled=True)
    gate_pre = jnp.dot(arrived, gate_local, preferred_element_type=jnp.float32)
    up_pre = jnp.dot(arrived, up_local, preferred_element_type=jnp.float32)
    hidden = (jax.nn.silu(gate_pre) * up_pre).astype(jnp.bfloat16)
    partial_term = jnp.dot(hidden, down_local, preferred_element_type=jnp.float32)
    summed = lax.psum_scatter(
        partial_term.astype(jnp.bfloat16), "tp", scatter_dimension=1, tiled=True
    )
    returned = lax.all_to_all(summed, "ep", split_axis=0, concat_axis=0, tiled=True)
    picked = (
        jnp.take(returned, slot_of, axis=0)
        .reshape(row_count, top_count, returned.shape[1])
        .astype(jnp.float32)
    )
    combined = jnp.sum(picked * expert_weights[:, :, None], axis=1)
    squares = lax.psum(jnp.sum(combined * combined, axis=1), "tp")
    scaled = combined * lax.rsqrt(squares / D + EPS)[:, None] * out_gain
    return scaled.astype(jnp.bfloat16)


def per_device(
    query_rows,
    key_rows,
    value_rows,
    query_gain,
    key_gain,
    w_out,
    mixer_gain,
    expert_input,
    expert_ids,
    expert_weights,
    input_gain,
    w_gate,
    w_up,
    w_down,
    out_gain,
):
    mixer_result = mixer_half(
        query_rows, key_rows, value_rows, query_gain, key_gain, w_out, mixer_gain
    )
    moe_result = expert_half(
        expert_input, expert_ids, expert_weights, input_gain, w_gate, w_up, w_down, out_gain
    )
    return (mixer_result, moe_result)


def solution(mesh):
    return jax.shard_map(
        per_device,
        mesh=mesh,
        in_specs=(
            P("ep", "tp"),
            P("ep", "tp"),
            P("ep", "tp"),
            P(),
            P(),
            P("tp", None),
            P(),
            P("ep", None),
            P("ep", None),
            P("ep", None),
            P(),
            P("ep", None, "tp"),
            P("ep", None, "tp"),
            P("ep", "tp", None),
            P("tp"),
        ),
        out_specs=(P(("ep", "tp"), None), P("ep", "tp")),
        check_vma=False,
    )
```

profile of v0, /device:TPU:0, one launch (start us, length us, event | category | flops | bytes accessed | tf_op | source)
XLA Modules:
  0.0 311.4 jit_solution(17613963774754394233)
XLA Ops:
  8.1 1.2 reshape.323
  9.9 0.5 multiply_multiply_fusion.1
  10.4 1.4 multiply_cosine_fusion.1
  11.8 1.4 subtract_convert_fusion.3
  13.3 1.2 pad_maximum_fusion.1
  14.5 0.8 copy.79
  15.8 0.9 reduce-window.6
  17.3 2.9 scatter_custom_fusion
  21.0 3.4 %gather_fusion = bf16[576,2048]{1,0:T(8,128)(2,1)S(1)} fusion(bf16[193,2048]{1,0:T(8,128)(2,1)S(1)} %concatenate.13, s32[1024]{0:T(1024)S(1)} %pad_clamp_fusion.1), kind=kCustom, calls=%fused_computation | custom fusion | bytes 4720896 | tf_op jit(solution)/shard_map/jit(_take)/gather | solution.py:147
  24.4 1.8 broadcast_select_fusion
  26.2 7.4 %all-to-all-start = ((bf16[8,72,2048]{2,1,0:T(8,128)(2,1)}), bf16[8,72,2048]{2,1,0:T(8,128)(2,1)}, u32[]{:S(2)}, u32[]{:S(2)}) async-start(bf16[8,72,2048]{2,1,0:T(8,128)(2,1)} %broadcast_select_fusion), calls=%async_computation.1 | async-start | bytes 4718592 | tf_op jit(solution)/shard_map/all_to_all | solution.py:148
  33.6 0.7 all-gather.5.cloned.1.call-update
  35.1 1.2 multiply_reduce_fusion
  36.3 1.0 copy.54
  37.3 0.8 copy.55
  38.2 1.4 multiply_multiply_fusion
  39.6 2.5 subtract_convert_fusion.1
  42.0 1.0 pad_maximum_fusion
  43.2 75.3 %all-to-all-done = bf16[8,72,2048]{2,1,0:T(8,128)(2,1)} async-done(((bf16[8,72,2048]{2,1,0:T(8,128)(2,1)}), bf16[8,72,2048]{2,1,0:T(8,128)(2,1)}, u32[]{:S(2)}, u32[]{:S(2)}) %all-to-all-start) | async-done | bytes 2359328 | tf_op jit(solution)/shard_map/all_to_all | solution.py:148
  118.5 7.0 %fusion.17 = f32[576,1024]{1,0:T(8,128)} fusion(bf16[576,2048]{1,0:T(8,128)(2,1)} %bitcast.9, bf16[1,2048,1024]{2,1,0:T(8,128)(2,1)} %param.28), kind=kOutput, calls=%fused_computation.27 | convolution fusion | flops 2415919104 | bytes 8912896 | tf_op jit(solution)/shard_map/dot_general | solution.py:149
  125.5 11.7 %fusion.19 = bf16[576,2048]{1,0:T(8,128)(2,1)} fusion(bf16[1,1024,2048]{2,1,0:T(8,128)(2,1)} %param.30, f32[576,1024]{1,0:T(8,128)} %fusion.17, bf16[576,2048]{1,0:T(8,128)(2,1)} %bitcast.9, bf16[1,2048,1024]{2,1,0:T(8,128)(2,1)} %param.29), kind=kOutput, calls=%fused_computation.29 | convolution fusion | flops 4836556800 | bytes 15466496 | tf_op jit(solution)/shard_map/dot_general | solution.py:152
  137.5 5.7 %reshape.313 = bf16[6,512,4,128]{3,2,1,0:T(4,128)(2,1)} reshape(bf16[3072,512]{1,0:T(8,128)(2,1)} %all-gather.3.cloned.1.call-done) | data formatting | bytes 6291456 | tf_op jit(solution)/shard_map/reshape | solution.py:94
  143.1 35.7 %all-gather.5.cloned.1.call-done = bf16[3072,512]{1,0:T(8,128)(2,1)} async-done(((bf16[384,512]{1,0:T(8,128)(2,1)}), bf16[3072,512]{1,0:T(8,128)(2,1)}) %all-gather.5.cloned.1.call-update) | async-done | bytes 3145744 | tf_op jit(solution)/shard_map/all_gather | solution.py:90
  178.8 5.5 %reshape.317 = bf16[6,512,4,128]{3,2,1,0:T(4,128)(2,1)} reshape(bf16[3072,512]{1,0:T(8,128)(2,1)} %all-gather.5.cloned.1.call-done) | data formatting | bytes 6291456 | tf_op jit(solution)/shard_map/reshape | solution.py:95
  184.3 73.2 %while.15 = (s32[]{:T(128)}, f32[4,768]{1,0:T(4,128)S(1)}, f32[4,768]{1,0:T(4,128)S(1)}, f32[4,768,128]{2,1,0:T(8,128)S(1)}, bf16[6,512,4,128]{3,2,1,0:T(4,128)(...) while((s32[]{:T(128)}, f32[4,768]{1,0:T(4,128)S(1)}, ...), condition=%wide.region_5.6_spmd.clone, body=%wide.region_2.5_spmd.clone.sunk | while | flops 819084288 | bytes 51314824 | solution.py:96
  184.3 1.6 constant_dynamic-slice_fusion.3
  185.9 3.7 %bitcast_reduce_fusion.2 = (f32[4,768]{1,0:T(4,128)S(1)}, f32[4,512,768]{2,1,0:T(8,128)}) fusion(bf16[4,768,128]{2,1,0:T(8,128)(2,1)S(1)} %get-tuple-element.212, bf16[1,512,4,128]{3,2,1,0:T(4,128)(2,1)S(1)} %get-tuple-element.183), kind=kOutput, calls=%fused_computation.4.clone.1 | convolution fusion | flops 405795840 | bytes 7614464 | tf_op jit(solution)/shard_map/while/body/eval_jaxpr/gqd,ngd->gqn/dot_general | solution.py:68
  189.6 4.0 %fusion.59 = f32[4,768]{1,0:T(4,128)S(1)} fusion(f32[4,512,768]{2,1,0:T(8,128)} %get-tuple-element.185, f32[4,768]{1,0:T(4,128)S(1)} %select_maximum_fusion.2), kind=kLoop, calls=%fused_computation.7.clone.1 | loop fusion | flops 4715520 | bytes 6316032 | tf_op jit(solution)/shard_map/while/body/eval_jaxpr/reduce_sum | solution.py:74
  193.6 0.6 copy-done
  194.2 2.3 fusion.61
  196.5 1.6 constant_dynamic-slice_fusion.3
  198.1 3.7 %bitcast_reduce_fusion.2 = (f32[4,768]{1,0:T(4,128)S(1)}, f32[4,512,768]{2,1,0:T(8,128)}) fusion(bf16[4,768,128]{2,1,0:T(8,128)(2,1)S(1)} %get-tuple-element.212, bf16[1,512,4,128]{3,2,1,0:T(4,128)(2,1)S(1)} %get-tuple-element.183), kind=kOutput, calls=%fused_computation.4.clone.1 | convolution fusion | flops 405795840 | bytes 7614464 | tf_op jit(solution)/shard_map/while/body/eval_jaxpr/gqd,ngd->gqn/dot_general | solution.py:68
  201.8 4.0 %fusion.59 = f32[4,768]{1,0:T(4,128)S(1)} fusion(f32[4,512,768]{2,1,0:T(8,128)} %get-tuple-element.185, f32[4,768]{1,0:T(4,128)S(1)} %select_maximum_fusion.2), kind=kLoop, calls=%fused_computation.7.clone.1 | loop fusion | flops 4715520 | bytes 6316032 | tf_op jit(solution)/shard_map/while/body/eval_jaxpr/reduce_sum | solution.py:74
  205.8 0.6 copy-done
  206.4 2.3 fusion.61
  208.7 1.6 constant_dynamic-slice_fusion.3
  210.3 3.7 %bitcast_reduce_fusion.2 = (f32[4,768]{1,0:T(4,128)S(1)}, f32[4,512,768]{2,1,0:T(8,128)}) fusion(bf16[4,768,128]{2,1,0:T(8,128)(2,1)S(1)} %get-tuple-element.212, bf16[1,512,4,128]{3,2,1,0:T(4,128)(2,1)S(1)} %get-tuple-element.183), kind=kOutput, calls=%fused_computation.4.clone.1 | convolution fusion | flops 405795840 | bytes 7614464 | tf_op jit(solution)/shard_map/while/body/eval_jaxpr/gqd,ngd->gqn/dot_general | solution.py:68
  214.0 4.0 %fusion.59 = f32[4,768]{1,0:T(4,128)S(1)} fusion(f32[4,512,768]{2,1,0:T(8,128)} %get-tuple-element.185, f32[4,768]{1,0:T(4,128)S(1)} %select_maximum_fusion.2), kind=kLoop, calls=%fused_computation.7.clone.1 | loop fusion | flops 4715520 | bytes 6316032 | tf_op jit(solution)/shard_map/while/body/eval_jaxpr/reduce_sum | solution.py:74
  218.0 0.6 copy-done
  218.6 2.3 fusion.61
  220.9 1.6 constant_dynamic-slice_fusion.3
  222.5 3.7 %bitcast_reduce_fusion.2 = (f32[4,768]{1,0:T(4,128)S(1)}, f32[4,512,768]{2,1,0:T(8,128)}) fusion(bf16[4,768,128]{2,1,0:T(8,128)(2,1)S(1)} %get-tuple-element.212, bf16[1,512,4,128]{3,2,1,0:T(4,128)(2,1)S(1)} %get-tuple-element.183), kind=kOutput, calls=%fused_computation.4.clone.1 | convolution fusion | flops 405795840 | bytes 7614464 | tf_op jit(solution)/shard_map/while/body/eval_jaxpr/gqd,ngd->gqn/dot_general | solution.py:68
  226.2 4.0 %fusion.59 = f32[4,768]{1,0:T(4,128)S(1)} fusion(f32[4,512,768]{2,1,0:T(8,128)} %get-tuple-element.185, f32[4,768]{1,0:T(4,128)S(1)} %select_maximum_fusion.2), kind=kLoop, calls=%fused_computation.7.clone.1 | loop fusion | flops 4715520 | bytes 6316032 | tf_op jit(solution)/shard_map/while/body/eval_jaxpr/reduce_sum | solution.py:74
  230.2 0.6 copy-done
  230.8 2.3 fusion.61
  233.1 1.6 constant_dynamic-slice_fusion.3
  234.7 3.7 %bitcast_reduce_fusion.2 = (f32[4,768]{1,0:T(4,128)S(1)}, f32[4,512,768]{2,1,0:T(8,128)}) fusion(bf16[4,768,128]{2,1,0:T(8,128)(2,1)S(1)} %get-tuple-element.212, bf16[1,512,4,128]{3,2,1,0:T(4,128)(2,1)S(1)} %get-tuple-element.183), kind=kOutput, calls=%fused_computation.4.clone.1 | convolution fusion | flops 405795840 | bytes 7614464 | tf_op jit(solution)/shard_map/while/body/eval_jaxpr/gqd,ngd->gqn/dot_general | solution.py:68
  238.4 4.0 %fusion.59 = f32[4,768]{1,0:T(4,128)S(1)} fusion(f32[4,512,768]{2,1,0:T(8,128)} %get-tuple-element.185, f32[4,768]{1,0:T(4,128)S(1)} %select_maximum_fusion.2), kind=kLoop, calls=%fused_computation.7.clone.1 | loop fusion | flops 4715520 | bytes 6316032 | tf_op jit(solution)/shard_map/while/body/eval_jaxpr/reduce_sum | solution.py:74
  242.4 0.6 copy-done
  243.0 2.3 fusion.61
  245.3 1.6 constant_dynamic-slice_fusion.3
  246.9 3.7 %bitcast_reduce_fusion.2 = (f32[4,768]{1,0:T(4,128)S(1)}, f32[4,512,768]{2,1,0:T(8,128)}) fusion(bf16[4,768,128]{2,1,0:T(8,128)(2,1)S(1)} %get-tuple-element.212, bf16[1,512,4,128]{3,2,1,0:T(4,128)(2,1)S(1)} %get-tuple-element.183), kind=kOutput, calls=%fused_computation.4.clone.1 | convolution fusion | flops 405795840 | bytes 7614464 | tf_op jit(solution)/shard_map/while/body/eval_jaxpr/gqd,ngd->gqn/dot_general | solution.py:68
  250.6 4.0 %fusion.59 = f32[4,768]{1,0:T(4,128)S(1)} fusion(f32[4,512,768]{2,1,0:T(8,128)} %get-tuple-element.185, f32[4,768]{1,0:T(4,128)S(1)} %select_maximum_fusion.2), kind=kLoop, calls=%fused_computation.7.clone.1 | loop fusion | flops 4715520 | bytes 6316032 | tf_op jit(solution)/shard_map/while/body/eval_jaxpr/reduce_sum | solution.py:74
  254.6 0.6 copy-done
  255.2 2.3 fusion.61
  258.4 5.2 %convolution_convert_fusion = bf16[384,2048]{1,0:T(8,128)(2,1)} fusion(bf16[384,1024]{0,1:T(8,128)(2,1)S(1)} %bitcast.89, bf16[1024,2048]{1,0:T(8,128)(2,1)} %param.22), kind=kOutput, calls=%fused_computation.30 | convolution fusion | flops 1611399168 | bytes 6553600 | tf_op jit(solution)/shard_map/dot_general | solution.py:105
  263.8 3.6 %all-to-all-start.1 = ((bf16[8,72,512]{2,1,0:T(8,128)(2,1)}), bf16[8,72,512]{2,1,0:T(8,128)(2,1)S(1)}, u32[]{:S(2)}, u32[]{:S(2)}) async-start(bf16[8,72,512]{2,1,0:T(8,128)(2,1)} %bitcast.90), calls=%async_computation.3 | async-start | bytes 1179648 | tf_op jit(solution)/shard_map/all_to_all | solution.py:156
  267.7 22.6 %reduce-scatter.3.cloned.1.call-done = bf16[96,2048]{1,0:T(8,128)(2,1)} async-done(((bf16[384,2048]{1,0:T(8,128)(2,1)}), bf16[96,2048]{1,0:T(8,128)(2,1)}) %reduce-scatter.3.cloned.1.call-update) | async-done | bytes 393232 | tf_op jit(solution)/shard_map/reduce_scatter | solution.py:104
  290.3 1.2 fusion.29
  291.5 1.9 fusion.31
  293.4 2.1 gather_fusion.1
  295.6 1.6 multiply_reduce_fusion.1
  297.4 5.8 %psum.7 = f32[192]{0:T(256)S(1)} all-reduce(f32[192]{0:T(256)S(1)} %multiply_reduce_fusion.3), channel_id=1, replica_groups=mesh['ep'=8,'tp'=4] {'tp'}, use_global_device_ids=true, to_apply=%region_16.17 | all-reduce | flops 192 | bytes 1536 | tf_op jit(solution)/shard_map/psum | solution.py:163
  303.2 0.8 multiply_convert_fusion.1
  (101 shorter events, 5.4 us)
Async XLA Ops:
  8.0 1.9 copy-start.11
  8.0 129.4 %all-gather.3.cloned.1.call-start = ((), (), s32[]{:S(2)}) async-start(), calls=%async_computation.4 | async-start | bytes 3538944 | tf_op jit(solution)/shard_map/all_gather | solution.py:89
  11.8 1.5 copy-start.2
  11.8 1.5 copy-start.3
  11.8 1.5 copy-start.4
  13.3 2.1 copy-start.6
  13.3 7.1 %copy-start.1 = (bf16[192,2048]{1,0:T(8,128)(2,1)S(1)}, bf16[192,2048]{1,0:T(8,128)(2,1)}, u32[]{:S(2)}) copy-start(bf16[192,2048]{1,0:T(8,128)(2,1)} %param.24) | copy-start | bytes 2359300
  13.3 7.3 %copy-start.7 = (f32[2048]{0:T(1024)S(1)}, f32[2048]{0:T(1024)}, u32[]{:S(2)}) copy-start(f32[2048]{0:T(1024)} %param.27) | copy-start | bytes 24580
  26.2 8.4 %copy-start.5 = (bf16[384,1024]{1,0:T(8,128)(2,1)S(1)}, bf16[384,1024]{1,0:T(8,128)(2,1)}, u32[]{:S(2)}) copy-start(bf16[384,1024]{1,0:T(8,128)(2,1)} %param.17) | copy-start | bytes 2359300
  26.2 92.3 %all-to-all-start = ((bf16[8,72,2048]{2,1,0:T(8,128)(2,1)}), bf16[8,72,2048]{2,1,0:T(8,128)(2,1)}, u32[]{:S(2)}, u32[]{:S(2)}) async-start(bf16[8,72,2048]{2,1,0:T(8,128)(2,1)} %broadcast_select_fusion), calls=%async_computation.1 | async-start | bytes 4718592 | tf_op jit(solution)/shard_map/all_to_all | solution.py:148
  33.6 145.2 %all-gather.5.cloned.1.call-start = ((), (), s32[]{:S(2)}) async-start(), calls=%async_computation.5 | async-start | bytes 3538944 | tf_op jit(solution)/shard_map/all_gather | solution.py:90
  34.3 229.5 %reduce-scatter.5.cloned.1.call-start = ((), (), s32[]{:S(2)}) async-start(), calls=%async_computation.7 | async-start | bytes 2949120 | tf_op jit(solution)/shard_map/reduce_scatter | solution.py:153
  34.8 3.4 %copy-start.12 = (f32[128]{0:T(128)S(1)}, f32[128]{0:T(128)}, u32[]{:S(2)}) copy-start(f32[128]{0:T(128)} %param.20) | copy-start | bytes 1540
  137.2 153.2 %reduce-scatter.3.cloned.1.call-start = ((), (), s32[]{:S(2)}) async-start(), calls=%async_computation.6 | async-start | bytes 1966080 | tf_op jit(solution)/shard_map/reduce_scatter | solution.py:104
  189.6 4.6 %copy-start = (f32[4,512,768]{2,1,0:T(8,128)S(1)}, f32[4,512,768]{2,1,0:T(8,128)}, u32[]{:S(2)}) copy-start(f32[4,512,768]{2,1,0:T(8,128)} %get-tuple-element.185) | copy-start | bytes 18874372 | tf_op jit(solution)/shard_map/while
  201.8 4.6 %copy-start = (f32[4,512,768]{2,1,0:T(8,128)S(1)}, f32[4,512,768]{2,1,0:T(8,128)}, u32[]{:S(2)}) copy-start(f32[4,512,768]{2,1,0:T(8,128)} %get-tuple-element.185) | copy-start | bytes 18874372 | tf_op jit(solution)/shard_map/while
  214.0 4.6 %copy-start = (f32[4,512,768]{2,1,0:T(8,128)S(1)}, f32[4,512,768]{2,1,0:T(8,128)}, u32[]{:S(2)}) copy-start(f32[4,512,768]{2,1,0:T(8,128)} %get-tuple-element.185) | copy-start | bytes 18874372 | tf_op jit(solution)/shard_map/while
  226.2 4.6 %copy-start = (f32[4,512,768]{2,1,0:T(8,128)S(1)}, f32[4,512,768]{2,1,0:T(8,128)}, u32[]{:S(2)}) copy-start(f32[4,512,768]{2,1,0:T(8,128)} %get-tuple-element.185) | copy-start | bytes 18874372 | tf_op jit(solution)/shard_map/while
  238.4 4.6 %copy-start = (f32[4,512,768]{2,1,0:T(8,128)S(1)}, f32[4,512,768]{2,1,0:T(8,128)}, u32[]{:S(2)}) copy-start(f32[4,512,768]{2,1,0:T(8,128)} %get-tuple-element.185) | copy-start | bytes 18874372 | tf_op jit(solution)/shard_map/while
  250.6 4.6 %copy-start = (f32[4,512,768]{2,1,0:T(8,128)S(1)}, f32[4,512,768]{2,1,0:T(8,128)}, u32[]{:S(2)}) copy-start(f32[4,512,768]{2,1,0:T(8,128)} %get-tuple-element.185) | copy-start | bytes 18874372 | tf_op jit(solution)/shard_map/while
  263.6 4.0 %copy-start.10 = (f32[192,2]{0,1:T(2,128)S(1)}, f32[192,2]{0,1:T(2,128)}, u32[]{:S(2)}) copy-start(f32[192,2]{0,1:T(2,128)} %param.26) | copy-start | bytes 4612
  263.6 27.9 %copy-start.8 = (f32[2048]{0:T(1024)S(1)}, f32[2048]{0:T(1024)}, u32[]{:S(2)}) copy-start(f32[2048]{0:T(1024)} %param.23) | copy-start | bytes 24580
  263.8 29.6 %all-to-all-start.1 = ((bf16[8,72,512]{2,1,0:T(8,128)(2,1)}), bf16[8,72,512]{2,1,0:T(8,128)(2,1)S(1)}, u32[]{:S(2)}, u32[]{:S(2)}) async-start(bf16[8,72,512]{2,1,0:T(8,128)(2,1)} %bitcast.90), calls=%async_computation.3 | async-start | bytes 1179648 | tf_op jit(solution)/shard_map/all_to_all | solution.py:156
  293.4 9.7 %copy-start.9 = (f32[512]{0:T(512)S(1)}, f32[512]{0:T(512)}, u32[]{:S(2)}) copy-start(f32[512]{0:T(512)} %param.31) | copy-start | bytes 6148
Sparse Core Ops, SparseCore 0:
  15.5 103.8 all-gather.2
  121.5 57.2 all-gather.4
Sparse Core Ops, SparseCore 1:
  137.2 32.1 reduce-scatter.4
  263.7 26.6 reduce-scatter.2
where the time goes:
time: 312 us; the launch traced here: 311 us
  waiting for transfers between devices  134 us (43%)
  matrix products  59.8 us (19%)
  other arithmetic  44.8 us (14%)
  local copies, waits for them, and re-layouts  38.9 us (12%)
  between operations  15.9 us (5%)
  starting transfers between devices  11.5 us (4%)
  blocking collectives  5.76 us (2%)
    all_to_all x1, waiting for transfers between devices, expert_half(): lax.all_to_all(outgoing, 'ep', split_axis=0, concat_axis=0, tiled=True)  75.3 us
    all_gather x1, waiting for transfers between devices, mixer_half(): value_piece = lax.all_gather(value_rows, 'ep', axis=0, tiled=True)  35.7 us
    reduce_sum x6, other arithmetic, attend_block(): running_sum = running_sum * factor + jnp.sum(exponent, axis=-1)  23.9 us
    reduce_scatter x1, waiting for transfers between devices, mixer_half(): lax.psum_scatter(jnp.dot(attended, w_out, preferred_element_type=jnp.floa...  22.6 us
    dot_general x6, matrix products, attend_block(): jnp.einsum('gqd,ngd->gqn', grouped, key_block, preferred_element_type=jnp...  22 us
    dot_general x6, matrix products, attend_block(): jnp.einsum('gqn,ngd->gqd', exponent.astype(jnp.bfloat16), value_block, pr...  14 us
    dot_general x1, matrix products, expert_half(): jnp.dot(hidden, down_local, preferred_element_type=jnp.float32)  11.7 us
    dynamic_slice x6, local copies, waits for them, and re-layouts, mixer_half(): carry, _ = lax.scan(attend_block, carry, (key_split, value_split))  9.39 us
  transfers between devices with their start and end apart: 6, of which 3 were waited for; matrix products, arithmetic and copies ran while one was open for 41% of the time, Pallas kernels for 0%

commit v1 on v0

v1 whole, which is shorter than its diff:
```python
import functools
import math

import jax
import jax.numpy as jnp
from jax import lax
from jax.experimental import pallas as pl
from jax.experimental.pallas import tpu as pltpu
from jax.sharding import PartitionSpec as P

D = 2048
GRID = 64
GROUPS = 4
BLOCK_Q = 384
BLOCK_K = 768


EPS = 1e-06
THETA = 10000.0


def turn_half(half_part, position):
    half_width = half_part.shape[-1]
    frequency = THETA ** (-jnp.arange(0, half_width, 2, dtype=jnp.float32) / half_width)
    angles = position[:, None, None] * frequency[None, None, :]
    cosine = jnp.cos(angles)
    sine_part = jnp.sin(angles)
    first_half = half_part[..., : half_width // 2]
    second = half_part[..., half_width // 2 :]
    return jnp.concatenate(
        [first_half * cosine - second * sine_part, second * cosine + first_half * sine_part],
        axis=-1,
    )


def norm_turn(raw_rows, gain_vec, row_offset):
    row_count = raw_rows.shape[0]
    head_dim = gain_vec.shape[0]
    head_count = raw_rows.shape[1] // head_dim
    by_head = raw_rows.astype(jnp.float32).reshape(row_count, head_count, head_dim)
    scaled = (
        by_head * lax.rsqrt(jnp.mean(by_head * by_head, axis=-1, keepdims=True) + EPS) * gain_vec
    )
    position = row_offset + jnp.arange(row_count, dtype=jnp.int32)
    grid_row = (position // GRID).astype(jnp.float32)
    grid_col = (position % GRID).astype(jnp.float32)
    half_dim = head_dim // 2
    turned = jnp.concatenate(
        [turn_half(scaled[..., :half_dim], grid_row), turn_half(scaled[..., half_dim:], grid_col)],
        axis=-1,
    )
    return turned.reshape(row_count, head_count * head_dim).astype(jnp.bfloat16)


def attend_kernel(scale, block_keys, q_ref, k_ref, v_ref, o_ref, vt_ref):
    @pl.when(pl.program_id(1) == 0)
    def _():
        vt_ref[...] = v_ref[...].T

    query = q_ref[...]
    columns = query.shape[0]
    head_dim = query.shape[1]
    steps = k_ref.shape[0] // block_keys

    def step(index, carry):
        top, total, acc = carry
        rows = pl.ds(pl.multiple_of(index * block_keys, block_keys), block_keys)
        scores = (
            lax.dot_general(
                k_ref[rows, :],
                query,
                (((1,), (1,)), ((), ())),
                preferred_element_type=jnp.float32,
            )
            * scale
        )
        new_top = jnp.maximum(top, jnp.max(scores, axis=0, keepdims=True))
        exponent = jnp.exp2(scores - new_top)
        factor = jnp.exp2(top - new_top)
        total = total * factor + jnp.sum(exponent, axis=0, keepdims=True)
        acc = acc * factor + jnp.dot(
            vt_ref[:, rows], exponent.astype(jnp.bfloat16), preferred_element_type=jnp.float32
        )
        return new_top, total, acc

    carry = (
        jnp.full((1, columns), -1e30, jnp.float32),
        jnp.zeros((1, columns), jnp.float32),
        jnp.zeros((head_dim, columns), jnp.float32),
    )
    if steps <= 8:
        for index in range(steps):
            carry = step(index, carry)
    else:
        carry = lax.fori_loop(0, steps, step, carry)
    _, total, acc = carry
    o_ref[...] = (acc / total).T.astype(o_ref.dtype)


def divisor(size, limit):
    block = limit
    while size % block:
        block -= 128
    return block


def attend(query, key, value, heads, head_dim, group_size, q_col, k_col, v_col):
    tokens = query.shape[0]
    keys = key.shape[0]
    block_q = divisor(tokens, BLOCK_Q)
    block_k = divisor(keys, BLOCK_K)
    flops = 4 * heads * tokens * keys * head_dim
    return pl.pallas_call(
        functools.partial(attend_kernel, head_dim**-0.5 * math.log2(math.e), block_k),
        grid=(heads, tokens // block_q),
        in_specs=[
            pl.BlockSpec((block_q, head_dim), lambda h, i: (i, q_col + h)),
            pl.BlockSpec((keys, head_dim), lambda h, i: (0, k_col + h // group_size)),
            pl.BlockSpec((keys, head_dim), lambda h, i: (0, v_col + h // group_size)),
        ],
        out_specs=pl.BlockSpec((block_q, head_dim), lambda h, i: (i, h)),
        out_shape=jax.ShapeDtypeStruct((tokens, heads * head_dim), jnp.bfloat16),
        scratch_shapes=[pltpu.VMEM((head_dim, keys), jnp.bfloat16)],
        compiler_params=pltpu.CompilerParams(dimension_semantics=("arbitrary", "arbitrary")),
        cost_estimate=pl.CostEstimate(
            flops=2 * flops,
            bytes_accessed=8 * tokens * heads * head_dim,
            transcendentals=heads * tokens * keys,
        ),
        name="attend",
    )(query, key, value)


def mixer_half(query_rows, key_rows, value_rows, query_gain, key_gain, w_out, mixer_gain):
    row_count = query_rows.shape[0]
    head_dim = query_gain.shape[0]
    n_ep = lax.axis_size("ep")
    row_offset = lax.axis_index("ep") * row_count
    query_turned = norm_turn(query_rows, query_gain, row_offset)
    key_turned = norm_turn(key_rows, key_gain, row_offset)
    local_heads = query_rows.shape[1] // head_dim
    group_size = query_rows.shape[1] // key_rows.shape[1]
    if local_heads == n_ep:
        by_head = [
            x.reshape(row_count, -1, head_dim).transpose(1, 0, 2)
            for x in (query_turned, key_turned, value_rows)
        ]
        outgoing = jnp.concatenate(
            [by_head[0]] + [jnp.repeat(x, group_size, axis=0) for x in by_head[1:]], axis=2
        )
        arrived = lax.all_to_all(outgoing, "ep", split_axis=0, concat_axis=0, tiled=True)
        packed = arrived.reshape(n_ep * row_count, 3 * head_dim)
        one_head = attend(packed, packed, packed, 1, head_dim, 1, 0, 1, 2)
        back = lax.all_to_all(
            one_head.reshape(n_ep, row_count, head_dim),
            "ep",
            split_axis=0,
            concat_axis=0,
            tiled=True,
        )
        attended = back.transpose(1, 0, 2).reshape(row_count, local_heads * head_dim)
    else:
        key_all = lax.all_gather(key_turned, "ep", axis=0, tiled=True)
        value_all = lax.all_gather(value_rows, "ep", axis=0, tiled=True)
        attended = attend(
            query_turned, key_all, value_all, local_heads, head_dim, group_size, 0, 0, 0
        )
    mixed_sum = lax.psum_scatter(
        jnp.dot(attended, w_out, preferred_element_type=jnp.float32).astype(jnp.bfloat16),
        "tp",
        scatter_dimension=0,
        tiled=True,
    ).astype(jnp.float32)
    scaled = (
        mixed_sum
        * lax.rsqrt(jnp.mean(mixed_sum * mixed_sum, axis=1, keepdims=True) + EPS)
        * mixer_gain
    )
    return scaled.astype(jnp.bfloat16)


def expert_half(
    expert_input, expert_ids, expert_weights, input_gain, w_gate, w_up, w_down, out_gain
):
    row_count, width = expert_input.shape
    top_count = expert_ids.shape[1]
    n_tp = lax.axis_size("tp")
    expert_total = w_gate.shape[0] * lax.axis_size("ep")
    inner_count = expert_total // GROUPS
    capacity = 3 * row_count // (4 * inner_count)
    slots = expert_total * capacity
    inputs_f = expert_input.astype(jnp.float32)
    normed = (
        inputs_f
        * lax.rsqrt(jnp.mean(inputs_f * inputs_f, axis=1, keepdims=True) + EPS)
        * input_gain
    ).astype(jnp.bfloat16)
    row_index = jnp.arange(row_count, dtype=jnp.int32)
    before = row_index[None, :] < row_index[:, None]
    slot_index = jnp.arange(slots, dtype=jnp.int32)
    slot_of = []
    for k in range(top_count):
        same = jnp.zeros((row_count, row_count), bool)
        for other in range(top_count):
            same = same | (expert_ids[:, k][:, None] == expert_ids[:, other][None, :])
        rank = jnp.sum((same & before).astype(jnp.int32), axis=1)
        slot_of.append(expert_ids[:, k] * capacity + rank)
    chosen = [slot_index[:, None] == slot[None, :] for slot in slot_of]
    picker = functools.reduce(jnp.logical_or, chosen).astype(jnp.bfloat16)
    share = width // n_tp
    own = lax.dynamic_slice_in_dim(normed, lax.axis_index("tp") * share, share, axis=1)
    outgoing = jnp.dot(picker, own, preferred_element_type=jnp.float32).astype(jnp.bfloat16)
    arrived = lax.all_to_all(
        outgoing.reshape(expert_total, capacity, share),
        "ep",
        split_axis=0,
        concat_axis=0,
        tiled=True,
    ).reshape(slots, share)
    shares = lax.all_gather(arrived, "tp", axis=0, tiled=False)
    arrived = jnp.concatenate([shares[j] for j in range(n_tp)], axis=1)
    gate_pre = jnp.dot(arrived, w_gate[0], preferred_element_type=jnp.float32)
    up_pre = jnp.dot(arrived, w_up[0], preferred_element_type=jnp.float32)
    hidden = (jax.nn.silu(gate_pre) * up_pre).astype(jnp.bfloat16)
    partial_term = jnp.dot(hidden, w_down[0], preferred_element_type=jnp.float32)
    summed = lax.psum_scatter(
        partial_term.astype(jnp.bfloat16), "tp", scatter_dimension=1, tiled=True
    )
    returned = lax.all_to_all(summed, "ep", split_axis=0, concat_axis=0, tiled=True)
    combined = jnp.zeros((row_count, returned.shape[1]), jnp.float32)
    for k in range(top_count):
        select = (slot_of[k][:, None] == slot_index[None, :]).astype(jnp.bfloat16)
        picked = jnp.dot(select, returned, preferred_element_type=jnp.float32)
        combined = combined + picked * expert_weights[:, k][:, None]
    squares = lax.psum(jnp.sum(combined * combined, axis=1), "tp")
    scaled = combined * lax.rsqrt(squares / D + EPS)[:, None] * out_gain
    return scaled.astype(jnp.bfloat16)


def per_device(
    query_rows,
    key_rows,
    value_rows,
    query_gain,
    key_gain,
    w_out,
    mixer_gain,
    expert_input,
    expert_ids,
    expert_weights,
    input_gain,
    w_gate,
    w_up,
    w_down,
    out_gain,
):
    mixer_result = mixer_half(
        query_rows, key_rows, value_rows, query_gain, key_gain, w_out, mixer_gain
    )
    moe_result = expert_half(
        expert_input, expert_ids, expert_weights, input_gain, w_gate, w_up, w_down, out_gain
    )
    return (mixer_result, moe_result)


def solution(mesh):
    return jax.shard_map(
        per_device,
        mesh=mesh,
        in_specs=(
            P("ep", "tp"),
            P("ep", "tp"),
            P("ep", "tp"),
            P(),
            P(),
            P("tp", None),
            P(),
            P("ep", None),
            P("ep", None),
            P("ep", None),
            P(),
            P("ep", None, "tp"),
            P("ep", None, "tp"),
            P("ep", "tp", None),
            P("tp"),
        ),
        out_specs=(P(("ep", "tp"), None), P("ep", "tp")),
        check_vma=False,
    )
```

time: 312 us -> 200 us (0.64)
  waiting for transfers between devices: 134 us -> 58.3 us
  blocking collectives: 5.76 us -> 53.3 us
  matrix products: 59.8 us -> 21.5 us
  other arithmetic: 44.8 us -> 10.8 us
  local copies, waits for them, and re-layouts: 38.9 us -> 11.3 us
  Pallas kernels: 0 us -> 22.7 us
  starting transfers between devices: 11.5 us -> 7.56 us
    all_to_all x1, waiting for transfers between devices: 75.3 us -> 25.9 us  [mixer_half(): lax.all_to_all(outgoing, 'ep', split_axis=0, concat_axis=0, tiled=True)]
    all_to_all x0 -> x2, blocking collectives: none -> 47.6 us  [the longest x1 23.8 us: expert_half(): lax.all_to_all(outgoing.reshape(expert_total, capacity, share), 'ep', spl...]
    dot_general x14 -> x5, matrix products: 54.6 us -> 16.3 us  [the longest x1 11 us: expert_half(): jnp.dot(hidden, w_down[0], preferred_element_type=jnp.float32)]
    all_gather x2 -> x1, waiting for transfers between devices: 35.7 us -> 8.87 us  [expert_half(): shares = lax.all_gather(arrived, 'tp', axis=0, tiled=False)]
    reduce_sum x9 -> x1, other arithmetic: 25.7 us -> 0.24 us  [expert_half(): rank = jnp.sum((same & before).astype(jnp.int32), axis=1)]
    pallas_call x0 -> x1, Pallas kernels: none -> 22.7 us  [attend(): pl.pallas_call(functools.partial(attend_kernel, head_dim ** (-0.5) * math...]
    reshape x3 -> x2, local copies, waits for them, and re-layouts: 11.3 us -> 1.58 us  [the longest x1 1.48 us: mixer_half(): one_head.reshape(n_ep, row_count, head_dim)]
    dynamic_slice x6 -> x1, local copies, waits for them, and re-layouts: 9.39 us -> 0.77 us  [expert_half(): lax.dynamic_slice_in_dim(normed, lax.axis_index('tp') * share, share, axi...]
  transfers between devices with their start and end apart: 6 -> 5, of which waited for: 3 -> 3; matrix products, arithmetic and copies ran while one was open for 41% -> 18% of each run, Pallas kernels for 0% -> 11%
where the time goes in v1:
time: 200 us
  waiting for transfers between devices  58.3 us (29%)
  blocking collectives  53.3 us (27%)
  Pallas kernels  22.7 us (11%)
  matrix products  21.5 us (11%)
  between operations  14.1 us (7%)
  local copies, waits for them, and re-layouts  11.3 us (6%)
  other arithmetic  10.8 us (5%)
  starting transfers between devices  7.56 us (4%)
    all_to_all x1, waiting for transfers between devices, mixer_half(): lax.all_to_all(outgoing, 'ep', split_axis=0, concat_axis=0, tiled=True)  25.9 us
    all_to_all x1, blocking collectives, expert_half(): lax.all_to_all(outgoing.reshape(expert_total, capacity, share), 'ep', spl...  23.8 us
    all_to_all x1, blocking collectives, mixer_half(): lax.all_to_all(one_head.reshape(n_ep, row_count, head_dim), 'ep', split_a...  23.7 us
    reduce_scatter x1, waiting for transfers between devices, mixer_half(): lax.psum_scatter(jnp.dot(attended, w_out, preferred_element_type=jnp.floa...  23.5 us
    pallas_call x1, Pallas kernels, attend(): pl.pallas_call(functools.partial(attend_kernel, head_dim ** (-0.5) * math...  22.7 us
    dot_general x1, matrix products, expert_half(): jnp.dot(hidden, w_down[0], preferred_element_type=jnp.float32)  11 us
    all_gather x1, waiting for transfers between devices, expert_half(): shares = lax.all_gather(arrived, 'tp', axis=0, tiled=False)  8.87 us
    psum x1, blocking collectives, expert_half(): squares = lax.psum(jnp.sum(combined * combined, axis=1), 'tp')  5.76 us
  transfers between devices with their start and end apart: 5, of which 3 were waited for; matrix products, arithmetic and copies ran while one was open for 18% of the time, Pallas kernels for 11%

profile of v1, /device:TPU:0, one launch (start us, length us, event | category | flops | bytes accessed | tf_op | source)
XLA Modules:
  0.0 199.7 jit_solution(8527189889655430641)
XLA Ops:
  7.2 0.0 all-gather.2.cloned.1.call-start
  7.2 1.4 convert_element_type.65
  8.6 0.0 copy-start.2
  8.6 0.2 multiply_reduce_fusion
  8.9 0.2 convert_reduce_fusion.1
  9.1 0.8 dynamic-slice
  9.9 0.4 convolution_convert_fusion.1
  10.3 0.0 copy-start.6
  10.3 23.8 %all_to_all.27 = bf16[8,72,512]{2,1,0:T(8,128)(2,1)} all-to-all(bf16[8,72,512]{2,1,0:T(8,128)(2,1)S(1)} %bitcast.67), channel_id=1, replica_groups=mesh['ep'=8,'tp'=4] {'ep'}, dimensions={0} | all-to-all | bytes 1179648 | tf_op jit(solution)/shard_map/all_to_all | solution.py:213
  34.2 0.0 all-gather.2.cloned.1.call-update
  34.2 0.0 copy-start.11
  34.2 0.4 copy.65
  34.6 0.4 multiply_cosine_fusion.1
  35.1 0.1 copy.70
  35.2 0.1 copy.71
  35.3 0.1 copy.72
  35.5 0.1 copy.73
  35.6 0.2 reshape.270
  35.9 0.5 multiply_reduce_fusion.1
  36.4 0.5 multiply_multiply_fusion
  36.9 1.4 subtract_convert_fusion.1
  38.3 0.0 copy-start.5
  38.3 0.0 copy-start.12
  38.4 1.2 maximum_bitcast_fusion.1
  39.6 0.3 copy.74
  39.9 0.1 reshape.261
  40.0 0.3 copy.75
  40.3 0.2 fusion.11
  40.5 0.2 fusion.12
  40.7 0.2 subtract_convert_fusion.3
  40.9 0.1 maximum_bitcast_fusion
  41.0 0.1 broadcast_in_dim.4
  41.1 0.1 broadcast_in_dim.5
  41.2 0.3 pad_maximum_fusion
  41.5 2.7 %copy.76 = bf16[8,384,384]{2,1,0:T(8,128)(2,1)} copy(bf16[8,384,384]{1,2,0:T(8,128)(2,1)S(1)} %pad_maximum_fusion) | data formatting | bytes 4718592 | tf_op jit(solution)/shard_map/concatenate | solution.py:148
  44.1 3.6 %all-to-all-start = ((bf16[8,384,384]{2,1,0:T(8,128)(2,1)}), bf16[8,384,384]{2,1,0:T(8,128)(2,1)S(1)}, u32[]{:S(2)}, u32[]{:S(2)}) async-start(bf16[8,384,384]{2,1,0:T(8,128)(2,1)} %copy.76), calls=%async_computation | async-start | bytes 4718592 | tf_op jit(solution)/shard_map/all_to_all | solution.py:151
  47.7 0.2 reduce-scatter.5.cloned.1.call-start
  48.0 8.9 %all-gather.2.cloned.1.call-done = bf16[4,576,512]{2,1,0:T(8,128)(2,1)} async-done(((bf16[1,576,512]{2,1,0:T(8,128)(2,1)}), bf16[4,576,512]{2,1,0:T(8,128)(2,1)}) %all-gather.2.cloned.1.call-update) | async-done | bytes 2359312 | tf_op jit(solution)/shard_map/all_gather | solution.py:220
  56.9 1.9 slice_bitcast_fusion.3
  58.8 0.8 copy-done.3
  59.6 0.2 copy-done.4
  59.8 0.1 copy-done.13
  59.8 4.1 %fusion.4 = f32[576,1024]{1,0:T(8,128)} fusion(bf16[1,2048,1024]{2,1,0:T(8,128)(2,1)S(1)} %copy-done.13, bf16[576,512]{1,0:T(8,128)(2,1)S(1)} %get-tuple-element.5, bf16[576,512]{1,0:T(8,128)(2,1)S(1)} %get-tuple-element.6, bf16[576,512]{1,0:T(8,128)(2,1)S(1)} %get-tuple-element.7, bf16[576,512]{1,0:T(8,128)(2,1)S(1)} %get-tuple-element.4), kind=kOutput, calls=%fused_computation.4 | convolution fusion | flops 2425356288 | bytes 8912896 | tf_op jit(solution)/shard_map/dot_general | solution.py:222
  63.9 11.0 %fusion.6 = bf16[576,2048]{1,0:T(8,128)(2,1)} fusion(bf16[1,1024,2048]{2,1,0:T(8,128)(2,1)} %param.28, f32[576,1024]{1,0:T(8,128)} %fusion.4, bf16[1,2048,1024]{2,1,0:T(8,128)(2,1)} %param.27, bf16[576,512]{1,0:T(8,128)(2,1)S(1)} %get-tuple-element.5, bf16[576,512]{1,0:T(8,128)(2,1)} %copy-done.3, bf16[576,512]{1,0:T(8,128)(2,1)} %copy-done.4, ...), kind=kOutput, calls=%fused_computation.6 | convolution fusion | flops 4845993984 | bytes 15466496 | tf_op jit(solution)/shard_map/dot_general | solution.py:225
  74.9 0.0 reduce-scatter.5.cloned.1.call-update
  75.0 0.0 reduce-scatter.3.cloned.1.call-start
  75.0 25.9 %all-to-all-done = bf16[8,384,384]{2,1,0:T(8,128)(2,1)S(1)} async-done(((bf16[8,384,384]{2,1,0:T(8,128)(2,1)}), bf16[8,384,384]{2,1,0:T(8,128)(2,1)S(1)}, u32[]{:S(2)}, u32[]{:S(2)}) %all-to-all-start) | async-done | bytes 2359328 | tf_op jit(solution)/shard_map/all_to_all | solution.py:151
  100.9 1.4 copy-done.1
  102.3 22.7 %attend.1 = bf16[3072,128]{1,0:T(8,128)(2,1)} custom-call(bf16[3072,384]{1,0:T(8,128)(2,1)} %bitcast.59, bf16[3072,384]{1,0:T(8,128)(2,1)} %bitcast.60, bf16[3072,384]{1,0:T(8,128)(2,1)} %bitcast.61), custom_call_target="tpu_custom_call" | custom-call | flops 9663676416 | bytes 3145728 | tf_op jit(solution)/shard_map/attend/pallas_call | solution.py:113
  125.0 1.5 copy.77
  126.5 23.7 %all_to_all.28 = bf16[8,384,128]{1,2,0:T(8,128)(2,1)S(1)} all-to-all(bf16[8,384,128]{1,2,0:T(8,128)(2,1)S(1)} %copy.77), channel_id=1, replica_groups=mesh['ep'=8,'tp'=4] {'ep'}, dimensions={0} | all-to-all | bytes 1572864 | tf_op jit(solution)/shard_map/all_to_all | solution.py:154
  150.2 5.2 %convolution_convert_fusion = bf16[384,2048]{1,0:T(8,128)(2,1)} fusion(bf16[384,1024]{0,1:T(8,128)(2,1)S(1)} %bitcast.65, bf16[1024,2048]{1,0:T(8,128)(2,1)} %param.20), kind=kOutput, calls=%fused_computation.7 | convolution fusion | flops 1611399168 | bytes 6553600 | tf_op jit(solution)/shard_map/dot_general | solution.py:169
  155.4 0.0 reduce-scatter.3.cloned.1.call-update
  155.4 0.0 reduce-scatter.5.cloned.1.call-done
  155.5 0.0 copy-start.9
  155.5 3.6 %all-to-all-start.3 = ((bf16[8,72,512]{2,1,0:T(8,128)(2,1)}), bf16[8,72,512]{2,1,0:T(8,128)(2,1)S(1)}, u32[]{:S(2)}, u32[]{:S(2)}) async-start(bf16[8,72,512]{2,1,0:T(8,128)(2,1)} %bitcast.66), calls=%async_computation.5 | async-start | bytes 1179648 | tf_op jit(solution)/shard_map/all_to_all | solution.py:229
  159.1 23.5 %reduce-scatter.3.cloned.1.call-done = bf16[96,2048]{1,0:T(8,128)(2,1)} async-done(((bf16[384,2048]{1,0:T(8,128)(2,1)}), bf16[96,2048]{1,0:T(8,128)(2,1)}) %reduce-scatter.3.cloned.1.call-update) | async-done | bytes 393232 | tf_op jit(solution)/shard_map/reduce_scatter | solution.py:168
  182.6 1.2 fusion.16
  183.8 1.9 fusion.18
  185.7 0.0 all-to-all-done.3
  185.7 0.4 convolution_multiply_fusion
  186.1 0.5 multiply_reduce_fusion.2
  186.6 5.8 %psum.7 = f32[192]{0:T(256)S(1)} all-reduce(f32[192]{0:T(256)S(1)} %get-tuple-element.32), channel_id=1, replica_groups=mesh['ep'=8,'tp'=4] {'tp'}, use_global_device_ids=true, to_apply=%region_9.10 | all-reduce | flops 192 | bytes 1536 | tf_op jit(solution)/shard_map/psum | solution.py:235
  192.3 0.8 multiply_convert_fusion.1
  (29 shorter events, 0.2 us)
Async XLA Ops:
  7.2 1.4 copy-start
  7.2 1.7 copy-start.8
  7.2 49.7 %all-gather.2.cloned.1.call-start = ((), (), s32[]{:S(2)}) async-start(), calls=%async_computation.7 | async-start | bytes 2949120 | tf_op jit(solution)/shard_map/all_gather | solution.py:220
  8.6 25.6 %copy-start.2 = (bf16[384,1024]{1,0:T(8,128)(2,1)S(1)}, bf16[384,1024]{1,0:T(8,128)(2,1)}, u32[]{:S(2)}) copy-start(bf16[384,1024]{1,0:T(8,128)(2,1)} %param.15) | copy-start | bytes 2359300
  10.3 25.3 %copy-start.6 = (bf16[384,512]{1,0:T(8,128)(2,1)S(1)}, bf16[384,512]{1,0:T(8,128)(2,1)}, u32[]{:S(2)}) copy-start(bf16[384,512]{1,0:T(8,128)(2,1)} %param.16) | copy-start | bytes 1179652
  34.2 2.2 %copy-start.11 = (f32[128]{0:T(128)S(1)}, f32[128]{0:T(128)}, u32[]{:S(2)}) copy-start(f32[128]{0:T(128)} %param.19) | copy-start | bytes 1540
  38.3 1.5 copy-start.5
  38.3 2.1 %copy-start.12 = (f32[128]{0:T(128)S(1)}, f32[128]{0:T(128)}, u32[]{:S(2)}) copy-start(f32[128]{0:T(128)} %param.18) | copy-start | bytes 1540
  44.1 56.7 %all-to-all-start = ((bf16[8,384,384]{2,1,0:T(8,128)(2,1)}), bf16[8,384,384]{2,1,0:T(8,128)(2,1)S(1)}, u32[]{:S(2)}, u32[]{:S(2)}) async-start(bf16[8,384,384]{2,1,0:T(8,128)(2,1)} %copy.76), calls=%async_computation | async-start | bytes 4718592 | tf_op jit(solution)/shard_map/all_to_all | solution.py:151
  47.7 107.7 %reduce-scatter.5.cloned.1.call-start = ((), (), s32[]{:S(2)}) async-start(), calls=%async_computation.8 | async-start | bytes 2949120 | tf_op jit(solution)/shard_map/reduce_scatter | solution.py:226
  56.9 3.0 %copy-start.13 = (bf16[1,2048,1024]{2,1,0:T(8,128)(2,1)S(1)}, bf16[1,2048,1024]{2,1,0:T(8,128)(2,1)}, u32[]{:S(2)}) copy-start(bf16[1,2048,1024]{2,1,0:T(8,128)(2,1)} %param.26) | copy-start | bytes 12582916
  58.8 0.8 copy-start.3
  58.8 1.0 copy-start.4
  75.0 107.7 %reduce-scatter.3.cloned.1.call-start = ((), (), s32[]{:S(2)}) async-start(), calls=%async_computation.6 | async-start | bytes 1966080 | tf_op jit(solution)/shard_map/reduce_scatter | solution.py:168
  100.9 1.4 copy-start.1
  155.4 3.7 %copy-start.10 = (f32[192,2]{0,1:T(2,128)S(1)}, f32[192,2]{0,1:T(2,128)}, u32[]{:S(2)}) copy-start(f32[192,2]{0,1:T(2,128)} %param.24) | copy-start | bytes 4612
  155.4 28.4 %copy-start.7 = (f32[2048]{0:T(1024)S(1)}, f32[2048]{0:T(1024)}, u32[]{:S(2)}) copy-start(f32[2048]{0:T(1024)} %param.21) | copy-start | bytes 24580
  155.5 36.9 %copy-start.9 = (f32[512]{0:T(512)S(1)}, f32[512]{0:T(512)}, u32[]{:S(2)}) copy-start(f32[512]{0:T(512)} %param.29) | copy-start | bytes 6148
  155.5 30.2 %all-to-all-start.3 = ((bf16[8,72,512]{2,1,0:T(8,128)(2,1)}), bf16[8,72,512]{2,1,0:T(8,128)(2,1)S(1)}, u32[]{:S(2)}, u32[]{:S(2)}) async-start(bf16[8,72,512]{2,1,0:T(8,128)(2,1)} %bitcast.66), calls=%async_computation.5 | async-start | bytes 1179648 | tf_op jit(solution)/shard_map/all_to_all | solution.py:229
Sparse Core Ops, SparseCore 0:
  34.3 22.4 all-gather.1
  75.1 32.7 reduce-scatter.4
  155.5 27.0 reduce-scatter.2
